TPU v7x, 256 devices: a whole 4x4x8 slice. The times are simulated.
256 devices in a mesh: sp: 64 (over z, x, core), tp: 4 (over y).
Axes of the slice: x: 4, y: 4, z: 8, core: 2. Of those that a mesh axis runs over, the one named last changes fastest.
Arguments:
- queries: bfloat16 [8192, 2048], P('sp', 'tp'), may hold values from -6 to 6
- keys: bfloat16 [8192, 512], P('sp', 'tp'), may hold values from -6 to 6
- values: bfloat16 [8192, 512], P('sp', 'tp'), may hold values from -6 to 6
- break_bias: float32 [16], P('tp'), as said below
- residual: bfloat16 [8192, 4096], P(('sp', 'tp')), may hold values from -6 to 6
- w_out: bfloat16 [2048, 4096], P('tp'), may hold values from -0.125 to 0.125
- ffn_gain: float32 [4096], replicated, may hold values from 0.1 to 1.9
- pick_ids: int32 [8192, 2], P('sp'), may hold values from 0 to 63, as said below
- pair_logit: float32 [8192], P('sp'), may hold values from -8 to 8
- w_gate: bfloat16 [64, 4096, 1024], P('sp', None, 'tp'), may hold values from -0.09375 to 0.09375
- w_up: bfloat16 [64, 4096, 1024], P('sp', None, 'tp'), may hold values from -0.09375 to 0.09375
- w_down: bfloat16 [64, 1024, 4096], P('sp', 'tp'), may hold values from -0.1875 to 0.1875
- out_gain: float32 [4096], replicated, may hold values from 0.1 to 1.9
Outputs:
- new_stream: bfloat16 [8192, 4096], P(('sp', 'tp'))
Inputs may be any that keep to these rules, and one draw needn't show every extreme that they name: `break_bias`: the logarithm of a break rate per position: between ln(0.02 / 8192) and ln(8 / 128). `pick_ids`: A row's 2 experts differ and lie in one group of 16 consecutive experts. In each aligned block of 32 rows no expert is named more than 2 times, and some expert exactly 2 times.
All inputs are finite; a program needn't handle non-finite values.
Results may differ from a plain program's by a relative error of at most 0.017.
Values may be sent and summed in bfloat16 or wider, within the bound.
A program may use at most 64 MiB of HBM per device.

v0:
```python
import functools

import jax
import jax.numpy as jnp
from jax import lax
from jax.experimental import pallas as pl
from jax.experimental.pallas import tpu as pltpu
from jax.sharding import PartitionSpec as P

LOG2E = 1.4426950408889634
KB = 256

def attend_block(qs, k_ref, v_ref, tri, bias_ref, acc, used, pair, masked, shift):
    k = jnp.concatenate([k_ref[0, pair], k_ref[1, pair]], axis=0)
    v = jnp.concatenate([v_ref[0, pair], v_ref[1, pair]], axis=0)
    s = lax.dot_general(qs[...], k, (((1,), (1,)), ((), ())), preferred_element_type=jnp.float32)
    rows = s.shape[0] // 4
    c = LOG2E * 128 ** -0.5
    zs, hl = [], []
    if masked:
        col = lax.broadcasted_iota(jnp.int32, (rows, KB), 1)
        row = lax.broadcasted_iota(jnp.int32, (rows, KB), 0)
        before = col < row + shift
    for h in range(4):
        z = s[h * rows:(h + 1) * rows] * c + bias_ref[0, h] * LOG2E
        b = jnp.maximum(z, 0.0) + jnp.log2(1.0 + jnp.exp2(-jnp.abs(z)))
        if masked:
            b = jnp.where(before, b, 0.0)
        zs.append(z)
        hl.append(b.astype(jnp.bfloat16))
    incl = jnp.dot(jnp.concatenate(hl, axis=0), tri[...], preferred_element_type=jnp.float32)
    ws = []
    for h in range(4):
        sl = slice(h * rows, (h + 1) * rows)
        u = used[sl]
        w = jnp.exp2(zs[h] - incl[sl] - jnp.concatenate([u, u], axis=1))
        if masked:
            w = jnp.where(before, w, 0.0)
        ws.append(w.astype(jnp.bfloat16))
        used[sl] = u + jnp.broadcast_to(incl[sl, 0:1], (rows, 128))
    acc[...] += jnp.dot(jnp.concatenate(ws, axis=0), v, preferred_element_type=jnp.float32)

MESH = pl.DeviceIdType.MESH
NZ, NX = 8, 4

def place():
    sp = lax.axis_index("sp")
    return sp // 8, (sp // 2) % 4, sp % 2

def device(z, x, c):
    return {"sp": z * 8 + x * 2 + c, "tp": lax.axis_index("tp")}

def gather_plan():
    zs = [("A", d) for d in (1, 2, 3, 4)] + [("B", d) for d in (1, 2, 3)]
    xs = [("A", 1), ("A", 2), ("B", 1)]
    none = ("O", 0)
    events = []
    for r in zs:
        events.append((r[1], "k", r, none, "z"))
    for rz in [none] + zs:
        for rx in xs:
            events.append((rz[1] + rx[1] + 0.25, "k", rz, rx, "x"))
    for r in xs:
        events.append((r[1], "v", none, r, "x"))
    for rx in [none] + xs:
        for rz in zs:
            events.append((rz[1] + rx[1] + 0.25, "v", rz, rx, "z"))
    return sorted(events)


def y_ring():
    y = lax.axis_index("tp")
    return y, (y + 1) % 4, (y + 3) % 4, (y + 2) % 4


OFFS = (0, 2, -2, 4, 3, -3, 1, -1)


def slot_columns(pick_ref, z):
    rows = lax.broadcasted_iota(jnp.int32, (128, 128), 0)
    lanes = lax.broadcasted_iota(jnp.int32, (128, 128), 1)
    earlier = (lanes < rows) & ((lanes & 96) == (rows & 96))
    across = [jnp.broadcast_to(pick_ref[k : k + 1, :], (128, 128)) for k in range(2)]
    wide = [w.astype(jnp.float32).T.astype(jnp.int32) for w in across]
    lane, late = [], []
    for w in wide:
        same = earlier & ((across[0] == w) | (across[1] == w))
        rank = jnp.sum(jnp.where(same, 1.0, 0.0), axis=1, keepdims=True).astype(jnp.int32)
        away = (z - (w >> 3)) & 7
        chunk = sum(jnp.where(away == (off & 7), o, 0) for o, off in enumerate(OFFS))
        lane.append((w & 7) * 16 + (chunk & 3) * 2 + rank)
        late.append(chunk >> 2)
    return lane, late


def layer_kernel(q_hbm, k_hbm, v_hbm, bias_hbm, res_hbm, w_hbm, gain_hbm, pick_hbm, logit_hbm, gate_hbm, up_hbm, down_ref, last_hbm,
                 out_ref,
                 q_ref, k_ref, v_ref, bias_ref, res_ref, w_ref, gain_ref, pick_ref, logit_ref, gate_ref, up_ref, last_ref,
                 stream_ref, disp_ref, down, kall, vall, qs, tri, acc, used, head, drelay, part, from_left, from_right, relay, summed, slots,
                 recv_x, send_z, got, hid, result, recv_r, send_x, recv_b, blend, send_f, fin,
                 ssem, rsem, dsend, drecv, msend, mrecv, xsend, xrecv, lsem):
    z, x, c = place()
    sp = lax.axis_index("sp")
    y, right, left, over = y_ring()
    sgn = 1 - 2 * c
    step = {"A": sgn, "B": -sgn, "O": 0}
    barrier = pltpu.get_barrier_semaphore()
    zn = {"A": (z + sgn + NZ) % NZ, "B": (z - sgn + NZ) % NZ}
    xn = {"A": (x + sgn + NX) % NX, "B": (x - sgn + NX) % NX}
    to_y = [{"sp": sp, "tp": t} for t in (right, left)]
    plane = [(z, (x + o // 2) % 4, (c + o) % 2) for o in range(8)]
    column = [((z + d) % 8, x, c) for d in range(8)]
    peers = [device(zn["A"], x, c), device(zn["B"], x, c), device(z, xn["A"], c), device(z, xn["B"], c), device(z, x, 1 - c)]
    for p in plane[1:] + column[1:]:
        pl.semaphore_signal(barrier, inc=1, device_id=device(*p), device_id_type=MESH)
    for t in (right, left, over):
        pl.semaphore_signal(barrier, inc=1, device_id={"sp": sp, "tp": t}, device_id_type=MESH)
    loads = {}
    for n, (name, src, dst) in enumerate((
        ("k", k_hbm, k_ref), ("v", v_hbm, v_ref), ("q", q_hbm, q_ref), ("bias", bias_hbm, bias_ref),
        ("picks", pick_hbm, pick_ref), ("w", w_hbm, w_ref), ("res", res_hbm, res_ref), ("gain", gain_hbm, gain_ref),
        ("gate", gate_hbm, gate_ref), ("up", up_hbm, up_ref), ("last", last_hbm, last_ref), ("logit", logit_hbm, logit_ref),
    )):
        loads[name] = pltpu.make_async_copy(src, dst, lsem.at[n + 1])
        loads[name].start()

    def columns(t):
        return pl.ds(pl.multiple_of(t * 1024, 1024), 1024)

    own_down = pltpu.make_async_copy(down_ref.at[:, columns(y)], down.at[y], lsem.at[0])
    own_down.start()
    loads["k"].wait()
    loads["v"].wait()
    pl.semaphore_wait(barrier, 17)

    def across(n, src, dst, to):
        return pltpu.make_async_remote_copy(src_ref=src, dst_ref=dst, send_sem=dsend.at[n], recv_sem=drecv.at[n], device_id=to_y[to], device_id_type=MESH)

    down_copies = [
        across(0, down_ref.at[0:128, columns(over)], drelay.at[0], 0),
        across(1, down_ref.at[128:256, columns(over)], drelay.at[1], 1),
        across(2, down_ref.at[:, columns(right)], down.at[y], 0),
        across(3, down_ref.at[:, columns(left)], down.at[y], 1),
    ]
    passed_on = [across(4, drelay.at[0], down.at[left, 0:128], 0), across(5, drelay.at[1], down.at[right, 128:256], 1)]
    down_arrivals = [
        across(2, down.at[left], down.at[left], 0), across(3, down.at[right], down.at[right], 1),
        across(4, down.at[over, 0:128], down.at[over, 0:128], 0), across(5, down.at[over, 128:256], down.at[over, 128:256], 1),
    ]
    zto = {"A": peers[0], "B": peers[1]}
    xto = {"A": peers[2], "B": peers[3]}
    full = {"k": kall, "v": vall}
    own = {"k": k_ref, "v": v_ref}
    tags = {}

    def tag(key):
        return tags.setdefault(key, len(tags))

    def source(rz, rx):
        return ((z - step[rz[0]] * rz[1] + NZ) % NZ) * NX + (x - step[rx[0]] * rx[1] + NX) % NX

    sends = []

    def send(arr, rz, rx, kind, to):
        i = source(rz, rx)
        src = own[arr] if (rz[1] == 0 and rx[1] == 0) else full[arr].at[c, i]
        if kind == "z":
            key, dst = (arr, (to, rz[1] + 1), rx, "z"), zto[to]
        elif kind == "x":
            key, dst = (arr, rz, (to, rx[1] + 1), "x"), xto[to]
        else:
            key, dst = (arr, rz, rx, "d"), peers[4]
        t = tag(key)
        copy = pltpu.make_async_remote_copy(src_ref=src, dst_ref=full[arr].at[c, i], send_sem=ssem.at[t], recv_sem=rsem.at[t], device_id=dst, device_id_type=MESH)
        copy.start()
        sends.append(copy)

    def arrived(arr, rz, rx, kind):
        t = tag((arr, rz, rx, kind))
        if kind == "d":
            i = ((z + step[rz[0]] * rz[1] + NZ) % NZ) * NX + (x + step[rx[0]] * rx[1] + NX) % NX
            ref = full[arr].at[1 - c, i]
        else:
            ref = full[arr].at[c, source(rz, rx)]
        pltpu.make_async_remote_copy(src_ref=ref, dst_ref=ref, send_sem=ssem.at[t], recv_sem=rsem.at[t], device_id=peers[4], device_id_type=MESH).wait_recv()

    most = {"A": 4, "B": 3}
    mostx = {"A": 2, "B": 1}
    o = ("O", 0)
    xs = [("A", 1), ("B", 1), ("A", 2)]
    send("k", o, o, "x", "A"); send("k", o, o, "x", "B"); send("v", o, o, "x", "A"); send("v", o, o, "x", "B")
    send("k", o, o, "d", None); send("v", o, o, "d", None)
    send("k", o, o, "z", "A"); send("k", o, o, "z", "B"); send("v", o, o, "z", "A"); send("v", o, o, "z", "B")
    me = z * NX + x
    kall[c, me] = k_ref[...]
    vall[c, me] = v_ref[...]
    loads["q"].wait()
    loads["bias"].wait()
    rows = q_ref.shape[0]
    for h in range(4):
        qs[h * rows:(h + 1) * rows] = q_ref[:, h * 128:(h + 1) * 128]
    r = lax.broadcasted_iota(jnp.int32, (KB, KB), 0)
    cc = lax.broadcasted_iota(jnp.int32, (KB, KB), 1)
    t = jnp.where(r >= cc, 1.0, 0.0).astype(jnp.bfloat16)
    tri[...] = t
    acc[...] = jnp.zeros_like(acc)
    used[...] = jnp.zeros_like(used)
    for it in down_copies:
        it.start()

    def receive(arr, rz, rx, kind):
        arrived(arr, rz, rx, kind)
        if kind == "z" and rz[1] < most[rz[0]]:
            send(arr, rz, rx, "z", rz[0])
        if kind == "x" and rx[1] < mostx[rx[0]]:
            send(arr, rz, rx, "x", rx[0])
        if arr == "k" and kind == "z":
            send(arr, rz, rx, "x", "A"); send(arr, rz, rx, "x", "B")
        if arr == "v" and kind == "x":
            send(arr, rz, rx, "z", "A"); send(arr, rz, rx, "z", "B")
        send(arr, rz, rx, "d", None)

    def ways(d):
        return [o] if d == 0 else [("A", d), ("B", d)] if d < 4 else [("A", 4)]

    def settle(d):
        for arr in "kv":
            for rx in [o] + xs:
                for rz in ways(d):
                    arrived(arr, rz, rx, "d")

    def block(d, i):
        if d == 0 and i == 0:
            attend_block(qs, kall, vall, tri, bias_ref, acc, used, me, True, c * rows)
        else:
            at = me - i if d == 0 else (z - d) * NX + 3 - i

            @pl.when(x >= i if d == 0 else z >= d)
            def _():
                attend_block(qs, kall, vall, tri, bias_ref, acc, used, at, False, 0)

    waiting = []
    plan = gather_plan()
    for n, (when, arr, rz, rx, kind) in enumerate(plan):
        if n == 20:
            for way in (0, 1):
                down_copies[way].wait_recv()
                passed_on[way].start()
        receive(arr, rz, rx, kind)
        if waiting and n % 2 == 1:
            waiting.pop(0)()
        if n + 1 == len(plan) or plan[n + 1][0] > when:
            d = when - 2.25
            if d in (0, 1, 2, 3):
                waiting.append(functools.partial(settle, int(d)))
                waiting.extend(functools.partial(block, int(d), i) for i in range(4))
    for step_of in waiting:
        step_of()
    settle(4)

    def rest(i, _):
        attend_block(qs, kall, vall, tri, bias_ref, acc, used, (z - 4) * NX + 3 - i, False, 0)
        return 0

    lax.fori_loop(0, jnp.where(z >= 4, (z - 3) * NX, 0), rest, 0)
    for h in range(4):
        a = acc[h * rows:(h + 1) * rows]
        sc = a * lax.rsqrt(jnp.mean(a * a, axis=-1, keepdims=True) + 1e-6)
        head[:, h * 128:(h + 1) * 128] = sc.astype(jnp.bfloat16)
    for it in down_arrivals:
        it.wait_recv()
    own_down.wait()
    loads["w"].wait()
    loads["res"].wait()
    loads["gain"].wait()
    loads["picks"].wait()
    def copy(n, src, dst, to):
        return pltpu.make_async_remote_copy(src_ref=src, dst_ref=dst, send_sem=msend.at[n], recv_sem=mrecv.at[n],
                                            device_id={"sp": sp, "tp": to}, device_id_type=MESH)

    def project(n):
        p = jnp.dot(head[...], w_ref[:, n * 1024:(n + 1) * 1024], preferred_element_type=jnp.float32).astype(jnp.bfloat16)
        for t in range(4):
            part[t, n // 2, :, (n % 2) * 1024:(n % 2 + 1) * 1024] = p[32 * t:32 * t + 32]

    copies = [
        copy(0, part.at[over, 0], relay.at[0], right),
        copy(1, part.at[over, 1], relay.at[1], left),
        copy(2, part.at[right, 1], from_left.at[1], right),
        copy(3, part.at[left, 0], from_right.at[0], left),
        copy(4, summed.at[0], from_left.at[0], right),
        copy(5, summed.at[1], from_right.at[1], left),
    ]
    project(0)
    project(1)
    copies[0].start()
    copies[3].start()
    project(2)
    project(3)
    copies[1].start()
    copies[2].start()
    lane, late = slot_columns(pick_ref, z)
    lanes = lax.broadcasted_iota(jnp.int32, (128, 128), 1)
    for h in range(2):
        for half in range(2):
            hit = [(lane[k] + 8 * half == lanes) & (late[k] == h) for k in range(2)]
            slots[h, half] = jnp.where(hit[0] | hit[1], 1.0, 0.0).astype(jnp.bfloat16)
    copies[0].wait_recv()
    summed[0] = (part[right, 0].astype(jnp.float32) + relay[0].astype(jnp.float32)).astype(jnp.bfloat16)
    copies[4].start()
    copies[1].wait_recv()
    summed[1] = (part[left, 1].astype(jnp.float32) + relay[1].astype(jnp.float32)).astype(jnp.bfloat16)
    copies[5].start()
    for n in (2, 3, 4, 5):
        copies[n].wait_recv()
    square = jnp.zeros((32, 1), jnp.float32)
    for h in range(2):
        cols = slice(h * 2048, (h + 1) * 2048)
        mixed = part[y, h].astype(jnp.float32) + from_left[h].astype(jnp.float32) + from_right[h].astype(jnp.float32)
        s = (res_ref[:, cols].astype(jnp.float32) + mixed).astype(jnp.bfloat16)
        stream_ref[:, cols] = s
        sf = s.astype(jnp.float32)
        square = square + jnp.sum(sf * sf, axis=1, keepdims=True)
    scale = lax.rsqrt(square * (1.0 / 4096) + 1e-6)
    tags_late = {}
    sent = []
    j = x * 2 + c
    bf, f32 = jnp.bfloat16, jnp.float32

    def late_copy(key, src, dst, to):
        n = tags_late.setdefault(key, len(tags_late))
        return pltpu.make_async_remote_copy(src_ref=src, dst_ref=dst, send_sem=xsend.at[n], recv_sem=xrecv.at[n],
                                            device_id=to, device_id_type=MESH)

    def push(key, src, dst, to):
        it = late_copy(key, src, dst, to)
        it.start()
        sent.append(it)

    def arrive(key, dst):
        late_copy(key, dst, dst, {"sp": sp, "tp": right}).wait_recv()

    way_y = {"R": {"sp": sp, "tp": right}, "L": {"sp": sp, "tp": left}, "O": {"sp": sp, "tp": over}}

    def pass_on_x(o, h):
        zz, xx, cc = plane[o]
        push(("x", o, h), disp_ref.at[h, xx * 2 + cc], recv_x.at[h, j], device(zz, xx, cc))

    own_rows = pl.ds(pl.multiple_of(y * 32, 32), 32)
    f = [(stream_ref[:, n * 2048:(n + 1) * 2048].astype(jnp.float32) * scale * gain_ref[:, n * 2048:(n + 1) * 2048]).astype(jnp.bfloat16) for n in range(2)]
    f = jnp.concatenate(f, axis=0)
    for h in range(2):
        mine = jnp.concatenate([slots[h, 0, own_rows, :], slots[h, 1, own_rows, :]], axis=0)
        d = lax.dot_general(mine, f, (((0,), (0,)), ((), ())), preferred_element_type=jnp.float32)
        disp_ref[h] = d.astype(jnp.bfloat16).reshape(8, 16, 2048)
        for o in (4, 5, 2, 3, 6, 7, 1):
            pass_on_x(o, h)
    loads["logit"].wait()
    logit = jnp.broadcast_to(logit_ref[...], (128, 128)).T
    second = ((lax.broadcasted_iota(jnp.int32, (128, 128), 0) >> 5) & 1) * 8
    chance = (jax.nn.sigmoid(logit), jax.nn.sigmoid(-logit))
    for h in range(2):
        w = sum(jnp.where((lane[k] + second == lanes) & (late[k] == h), chance[k], 0.0) for k in range(2))
        hi = w.astype(bf)
        blend[:, h * 128:(h + 1) * 128] = hi
        blend[:, 256 + h * 128:256 + (h + 1) * 128] = (w - hi.astype(f32)).astype(bf)
    a = lax.broadcasted_iota(jnp.int32, (128, 128), 0)
    b = lax.broadcasted_iota(jnp.int32, (128, 128), 1)
    outward = [jnp.where(b == ((a >> 1) & 7) * 16 + half * 8 + ((a >> 4) & 3) * 2 + (a & 1), 1.0, 0.0).astype(bf)[0:64] for half in range(2)]
    homeward = jnp.where(b == ((a >> 1) & 3) * 32 + ((a >> 3) & 1) * 16 + (a >> 4) * 2 + (a & 1), 1.0, 0.0).astype(bf)
    halves = [slice(0, 2048), slice(2048, 4096)]
    plane_order = (1, 2, 3, 6, 7, 4, 5)

    def place_of(o):
        return ((x - o // 2 + 4) % 4) * 2 + (c + o) % 2

    def over_y(o):
        for half in range(2):
            part = got.at[o, y, :, halves[half]]
            for way in "RL":
                push(("g", way, o, half), part, part, way_y[way])

    def permute(h):
        recv_x[h, j] = disp_ref[h, j]
        for o in plane_order:
            arrive(("x", o, h), recv_x.at[h, place_of(o)])
        v = recv_x[h].reshape(128, 2048)
        for half in range(2):
            p = jnp.dot(outward[half], v, preferred_element_type=f32).astype(bf).reshape(4, 16, 2048)
            send_z[4 * h:4 * h + 4, :, halves[half]] = p
            if h == 0:
                got[0, y, :, halves[half]] = p[0]
        for o in range(4 * h, 4 * h + 4):
            if o:
                push(("z", o), send_z.at[o], got.at[o, y], device((z - OFFS[o] + 8) % 8, x, c))
            else:
                over_y(0)

    def gather_own(g):
        for o in (2 * g, 2 * g + 1):
            if o:
                arrive(("z", o), got.at[o, y])
                over_y(o)

    def gather_on(g):
        for o in (2 * g, 2 * g + 1):
            for h, way, t in ((0, "R", left), (1, "L", right)):
                part = got.at[o, t, :, halves[h]]
                arrive(("g", way, o, h), part)
                push(("h", way, o), part, part, way_y[way])

    def hidden(g):
        for o in (2 * g, 2 * g + 1):
            arrive(("g", "R", o, 1), got.at[o, left, :, halves[1]])
            arrive(("g", "L", o, 0), got.at[o, right, :, halves[0]])
            arrive(("h", "R", o), got.at[o, over, :, halves[0]])
            arrive(("h", "L", o), got.at[o, over, :, halves[1]])
        v = got[2 * g:2 * g + 2].reshape(128, 4096)
        gate = jnp.dot(v, gate_ref[...], preferred_element_type=f32)
        up = jnp.dot(v, up_ref[...], preferred_element_type=f32)
        hid[g, y] = (gate / (1.0 + jnp.exp(-gate)) * up).astype(bf)
        for way in "RL":
            push(("u", way, g), hid.at[g, y], hid.at[g, y], way_y[way])

    def hidden_on(g):
        arrive(("u", "R", g), hid.at[g, left])
        half = hid.at[g, left, 0:64]
        push(("v", "R", g), half, half, way_y["R"])
        arrive(("u", "L", g), hid.at[g, right])
        half = hid.at[g, right, 64:128]
        push(("v", "L", g), half, half, way_y["L"])

    def outputs(g):
        arrive(("v", "R", g), hid.at[g, over, 0:64])
        arrive(("v", "L", g), hid.at[g, over, 64:128])
        h = jnp.concatenate([hid[g, t] for t in range(4)], axis=1)
        r = jnp.dot(h, down[...].reshape(1024, 1024), preferred_element_type=f32)
        result[2 * g:2 * g + 2] = r.astype(bf).reshape(2, 4, 16, 1024)
        for o in (2 * g, 2 * g + 1):
            if o:
                push(("r", o), result.at[o], recv_r.at[o], device((z + OFFS[o] + 8) % 8, x, c))
            else:
                recv_r[0] = result[0]

    def homeward_x(h):
        for o in range(4 * h, 4 * h + 4):
            if o:
                arrive(("r", o), recv_r.at[o])
        for t in range(2):
            v = recv_r[4 * h:4 * h + 4, 2 * t:2 * t + 2].reshape(128, 1024)
            p = jnp.dot(homeward, v, preferred_element_type=f32)
            send_x[h, :, t] = p.astype(bf).reshape(8, 16, 1024)
        for o in (4, 5, 2, 3, 6, 7, 1):
            zz, xx, cc = plane[o]
            push(("b", o, h), send_x.at[h, xx * 2 + cc], recv_b.at[h, j], device(zz, xx, cc))
        recv_b[h, j] = send_x[h, j]

    permute(0)
    permute(1)
    loads["gate"].wait()
    loads["up"].wait()
    loads["last"].wait()
    gather_own(0)
    for p in range(4):
        gather_on(p)
        if p > 0:
            hidden_on(p - 1)
        if p < 3:
            gather_own(p + 1)
        if p > 0:
            outputs(p - 1)
        hidden(p)
        if p == 3:
            homeward_x(0)
    hidden_on(3)
    outputs(3)
    homeward_x(1)
    for h in range(2):
        for o in plane_order:
            arrive(("b", o, h), recv_b.at[h, place_of(o)])

    def blended(t):
        w = blend[pl.ds(pl.multiple_of(t * 32, 32), 32), :]
        v = [recv_b[h, :, t // 2].reshape(128, 1024) for h in range(2)]
        v = jnp.concatenate(v + v, axis=0)
        return jnp.dot(w, v, preferred_element_type=f32).astype(bf)

    for way, t in (("O", over), ("R", right), ("L", left)):
        send_f[t] = blended(t)
        push(("f", way), send_f.at[t], fin.at[y], way_y[way])
    fin[y] = blended(y)
    for way, t in (("R", left), ("L", right), ("O", over)):
        arrive(("f", way), fin.at[t])
    square = jnp.zeros((32, 1), f32)
    for t in range(4):
        v = fin[t].astype(f32)
        square = square + jnp.sum(v * v, axis=1, keepdims=True)
    scale = lax.rsqrt(square * (1.0 / 4096) + 1e-6)
    for t in range(4):
        cols = slice(t * 1024, (t + 1) * 1024)
        out_ref[:, cols] = (stream_ref[:, cols].astype(f32) + fin[t].astype(f32) * scale * last_ref[:, cols]).astype(bf)
    for it in sends + down_copies + passed_on + copies + sent:
        it.wait_send()


def layer(*args):
    vm = pl.BlockSpec(memory_space=pltpu.VMEM)
    hbm = pl.BlockSpec(memory_space=pl.ANY)
    dma = pltpu.SemaphoreType.DMA
    bf, f32 = jnp.bfloat16, jnp.float32
    inputs = [((128, 512), bf), ((128, 128), bf), ((128, 128), bf)]
    late_inputs = [((32, 4096), bf), ((512, 4096), bf), ((1, 4096), f32), ((2, 128), jnp.int32), ((1, 128), f32),
                   ((4096, 256), bf), ((4096, 256), bf), ((1, 4096), f32)]
    sizes = [((32, 4096), bf), ((2, 8, 16, 2048), bf), ((4, 256, 1024), bf),
             ((2, 32, 128, 128), bf), ((2, 32, 128, 128), bf), ((512, 128), bf), ((KB, KB), bf), ((512, 128), f32),
             ((512, 128), f32), ((128, 512), bf), ((2, 128, 1024), bf), ((4, 2, 32, 2048), bf),
             ((2, 32, 2048), bf), ((2, 32, 2048), bf), ((2, 32, 2048), bf), ((2, 32, 2048), bf), ((2, 2, 128, 128), bf),
             ((2, 8, 16, 2048), bf), ((8, 16, 4096), bf), ((8, 4, 16, 4096), bf), ((4, 4, 128, 256), bf), ((8, 4, 16, 1024), bf),
             ((8, 4, 16, 1024), bf), ((2, 8, 2, 16, 1024), bf), ((2, 8, 2, 16, 1024), bf), ((128, 512), bf), ((4, 32, 1024), bf),
             ((4, 32, 1024), bf)]
    return pl.pallas_call(
        layer_kernel, out_shape=jax.ShapeDtypeStruct((32, 4096), bf), in_specs=[hbm] * 13, out_specs=vm,
        scratch_shapes=[pltpu.VMEM(*n) for n in inputs] + [pltpu.SMEM((1, 4), f32)] + [pltpu.VMEM(*n) for n in late_inputs + sizes]
        + [dma((126,)), dma((126,)), dma((6,)), dma((6,)), dma((6,)), dma((6,)), dma((112,)), dma((112,)), dma((13,))],
        compiler_params=pltpu.CompilerParams(collective_id=0, has_side_effects=True, vmem_limit_bytes=60 * 1024 * 1024),
    )(*args)


def on_device(
    queries, keys, values, break_bias, residual, w_out, ffn_gain, pick_ids, pair_logit, w_gate, w_up, w_down, out_gain
):
    return layer(
        queries, keys, values, break_bias.reshape(1, 4), residual, w_out, ffn_gain.reshape(1, -1), pick_ids.T,
        pair_logit.reshape(1, -1), w_gate[0], w_up[0], w_down[0], out_gain.reshape(1, -1)
    )


def solution(mesh):
    placed = (
        P("sp", "tp"),
        P("sp", "tp"),
        P("sp", "tp"),
        P("tp"),
        P(("sp", "tp"), None),
        P("tp", None),
        P(),
        P("sp", None),
        P("sp"),
        P("sp", None, "tp"),
        P("sp", None, "tp"),
        P("sp", "tp", None),
        P(),
    )
    return jax.shard_map(
        on_device, mesh=mesh, in_specs=placed, out_specs=P(("sp", "tp"), None), check_vma=False
    )
```

profile of v0, /device:TPU:1, one launch (start us, length us, event | category | flops | bytes accessed | tf_op | source)
XLA Modules:
  0.0 154.0 jit_solution(4508550014131531994)
XLA Ops:
  0.0 152.4 %shard_map.127 = bf16[32,4096]{1,0:T(8,128)(2,1)} custom-call(bf16[128,512]{1,0:T(8,128)(2,1)} %q_hbm.1, bf16[128,128]{1,0:T(8,128)(2,1)} %k_hbm.1, bf16[128,128]{1,0:T(8,128)(2,1)} %v_hbm.1, f32[1,4]{1,0:T(1,128)} %bitcast.14, bf16[32,4096]{1,0:T(8,128)(2,1)} %res_hbm.1, bf16[512,4096]{1,0:T(8,128)(2,1)} %w_hbm.1, f32[1,4096]{1,0:T(1,128)} %bitcast.11, ...), custom_call_target="tpu_custom_call" | custom-call | tf_op jit(solution)/shard_map/pallas_call | solution.py:521
  152.4 1.7 %copy.15 = bf16[32,4096]{1,0:T(8,128)(2,1)} copy(bf16[32,4096]{1,0:T(8,128)(2,1)} %shard_map.127) | data formatting | bytes 524288
where the time goes:
time: 154 us
  Pallas kernels  152 us (99%)
  local copies, waits for them, and re-layouts  1.67 us (1%)
    pallas_call x1, Pallas kernels, layer(): pl.pallas_call(layer_kernel, out_shape=jax.ShapeDtypeStruct((32, 4096), b...  152 us

commit v1 on v0

--- a/solution.py
+++ b/solution.py
@@ -10,35 +10,49 @@
 LOG2E = 1.4426950408889634
 KB = 256
 
-def attend_block(qs, k_ref, v_ref, tri, bias_ref, acc, used, pair, masked, shift):
-    k = jnp.concatenate([k_ref[0, pair], k_ref[1, pair]], axis=0)
-    v = jnp.concatenate([v_ref[0, pair], v_ref[1, pair]], axis=0)
-    s = lax.dot_general(qs[...], k, (((1,), (1,)), ((), ())), preferred_element_type=jnp.float32)
-    rows = s.shape[0] // 4
+def attend_blocks(qs, k_ref, v_ref, tri, bias_ref, acc, used, pairs, shift=None, behind=False):
+    rows = qs.shape[0] // 4
     c = LOG2E * 128 ** -0.5
-    zs, hl = [], []
-    if masked:
+    if shift is not None:
         col = lax.broadcasted_iota(jnp.int32, (rows, KB), 1)
         row = lax.broadcasted_iota(jnp.int32, (rows, KB), 0)
         before = col < row + shift
-    for h in range(4):
-        z = s[h * rows:(h + 1) * rows] * c + bias_ref[0, h] * LOG2E
-        b = jnp.maximum(z, 0.0) + jnp.log2(1.0 + jnp.exp2(-jnp.abs(z)))
-        if masked:
-            b = jnp.where(before, b, 0.0)
-        zs.append(z)
-        hl.append(b.astype(jnp.bfloat16))
-    incl = jnp.dot(jnp.concatenate(hl, axis=0), tri[...], preferred_element_type=jnp.float32)
-    ws = []
+    keys = [jnp.concatenate([k_ref[0, p], k_ref[1, p]], axis=0) for p in pairs]
+    vals = [jnp.concatenate([v_ref[0, p], v_ref[1, p]], axis=0) for p in pairs]
+    scores = [lax.dot_general(qs[...], k, (((1,), (1,)), ((), ())), preferred_element_type=jnp.float32) for k in keys]
+    zs, incls = [], []
+    for s in scores:
+        z_of, b_of = [], []
+        for h in range(4):
+            z = s[h * rows:(h + 1) * rows] * c + bias_ref[0, h] * LOG2E
+            b = jnp.maximum(z, 0.0) + jnp.log2(1.0 + jnp.exp2(-jnp.abs(z)))
+            if shift is not None:
+                b = jnp.where(before, b, 0.0)
+            z_of.append(z)
+            b_of.append(b.astype(jnp.bfloat16))
+        incls.append(jnp.dot(jnp.concatenate(b_of, axis=0), tri[...], preferred_element_type=jnp.float32))
+        zs.append(z_of)
+    gone = [jnp.zeros((rows, 128), jnp.float32) if behind else used[h * rows:(h + 1) * rows] for h in range(4)]
+    total = None
+    for z_of, incl, v in zip(zs, incls, vals):
+        ws = []
+        for h in range(4):
+            sl = slice(h * rows, (h + 1) * rows)
+            w = jnp.exp2(z_of[h] - incl[sl] - jnp.concatenate([gone[h], gone[h]], axis=1))
+            if shift is not None:
+                w = jnp.where(before, w, 0.0)
+            ws.append(w.astype(jnp.bfloat16))
+            gone[h] = gone[h] + jnp.broadcast_to(incl[sl, 0:1], (rows, 128))
+        part = jnp.dot(jnp.concatenate(ws, axis=0), v, preferred_element_type=jnp.float32)
+        total = part if total is None else total + part
     for h in range(4):
         sl = slice(h * rows, (h + 1) * rows)
-        u = used[sl]
-        w = jnp.exp2(zs[h] - incl[sl] - jnp.concatenate([u, u], axis=1))
-        if masked:
-            w = jnp.where(before, w, 0.0)
-        ws.append(w.astype(jnp.bfloat16))
-        used[sl] = u + jnp.broadcast_to(incl[sl, 0:1], (rows, 128))
-    acc[...] += jnp.dot(jnp.concatenate(ws, axis=0), v, preferred_element_type=jnp.float32)
+        if behind:
+            acc[sl] = total[sl] + jnp.exp2(-gone[h]) * acc[sl]
+        else:
+            acc[sl] += total[sl]
+            used[sl] = gone[h]
+
 
 MESH = pl.DeviceIdType.MESH
 NZ, NX = 8, 4
@@ -73,7 +87,7 @@
     return y, (y + 1) % 4, (y + 3) % 4, (y + 2) % 4
 
 
-OFFS = (0, 2, -2, 4, 3, -3, 1, -1)
+OFFS = (0, -3, 3, 2, -2, 4, 1, -1)
 
 
 def slot_columns(pick_ref, z):
@@ -97,7 +111,7 @@
                  out_ref,
                  q_ref, k_ref, v_ref, bias_ref, res_ref, w_ref, gain_ref, pick_ref, logit_ref, gate_ref, up_ref, last_ref,
                  stream_ref, disp_ref, down, kall, vall, qs, tri, acc, used, head, drelay, part, from_left, from_right, relay, summed, slots,
-                 recv_x, send_z, got, hid, result, recv_r, send_x, recv_b, blend, send_f, fin,
+                 recv_x, send_z, got, hid, result, recv_r, send_x, recv_b, blend, send_f, fin, far,
                  ssem, rsem, dsend, drecv, msend, mrecv, xsend, xrecv, lsem):
     z, x, c = place()
     sp = lax.axis_index("sp")
@@ -205,6 +219,7 @@
     tri[...] = t
     acc[...] = jnp.zeros_like(acc)
     used[...] = jnp.zeros_like(used)
+    far[...] = jnp.zeros_like(far)
     for it in down_copies:
         it.start()
 
@@ -231,13 +246,19 @@
 
     def block(d, i):
         if d == 0 and i == 0:
-            attend_block(qs, kall, vall, tri, bias_ref, acc, used, me, True, c * rows)
+            attend_blocks(qs, kall, vall, tri, bias_ref, acc, used, [me], c * rows)
         else:
             at = me - i if d == 0 else (z - d) * NX + 3 - i
 
             @pl.when(x >= i if d == 0 else z >= d)
             def _():
-                attend_block(qs, kall, vall, tri, bias_ref, acc, used, at, False, 0)
+                attend_blocks(qs, kall, vall, tri, bias_ref, acc, used, [at] if d == 0 else [at, at - 1])
+
+    def far_block(w, i):
+        @pl.when(z >= 8 - w)
+        def _():
+            at = (z + w - 8) * NX + 1 + i
+            attend_blocks(qs, kall, vall, tri, bias_ref, far, used, [at, at - 1], behind=True)
 
     waiting = []
     plan = gather_plan()
@@ -253,16 +274,18 @@
             d = when - 2.25
             if d in (0, 1, 2, 3):
                 waiting.append(functools.partial(settle, int(d)))
-                waiting.extend(functools.partial(block, int(d), i) for i in range(4))
+                waiting.extend(functools.partial(block, int(d), i) for i in (range(4) if d == 0 else (0, 2)))
+                if d:
+                    waiting.extend(functools.partial(far_block, int(d), i) for i in (0, 2))
     for step_of in waiting:
         step_of()
     settle(4)
 
-    def rest(i, _):
-        attend_block(qs, kall, vall, tri, bias_ref, acc, used, (z - 4) * NX + 3 - i, False, 0)
-        return 0
-
-    lax.fori_loop(0, jnp.where(z >= 4, (z - 3) * NX, 0), rest, 0)
+    @pl.when(z >= 4)
+    def _():
+        attend_blocks(qs, kall, vall, tri, bias_ref, acc, used, [(z - 4) * NX + 3 - n for n in range(4)])
+
+    acc[...] += jnp.exp2(-used[...]) * far[...]
     for h in range(4):
         a = acc[h * rows:(h + 1) * rows]
         sc = a * lax.rsqrt(jnp.mean(a * a, axis=-1, keepdims=True) + 1e-6)
@@ -467,12 +490,11 @@
             hidden_on(p - 1)
         if p < 3:
             gather_own(p + 1)
+        hidden(p)
         if p > 0:
             outputs(p - 1)
-        hidden(p)
-        if p == 3:
-            homeward_x(0)
     hidden_on(3)
+    homeward_x(0)
     outputs(3)
     homeward_x(1)
     for h in range(2):
@@ -517,7 +539,7 @@
              ((2, 32, 2048), bf), ((2, 32, 2048), bf), ((2, 32, 2048), bf), ((2, 32, 2048), bf), ((2, 2, 128, 128), bf),
              ((2, 8, 16, 2048), bf), ((8, 16, 4096), bf), ((8, 4, 16, 4096), bf), ((4, 4, 128, 256), bf), ((8, 4, 16, 1024), bf),
              ((8, 4, 16, 1024), bf), ((2, 8, 2, 16, 1024), bf), ((2, 8, 2, 16, 1024), bf), ((128, 512), bf), ((4, 32, 1024), bf),
-             ((4, 32, 1024), bf)]
+             ((4, 32, 1024), bf), ((512, 128), f32)]
     return pl.pallas_call(
         layer_kernel, out_shape=jax.ShapeDtypeStruct((32, 4096), bf), in_specs=[hbm] * 13, out_specs=vm,
         scratch_shapes=[pltpu.VMEM(*n) for n in inputs] + [pltpu.SMEM((1, 4), f32)] + [pltpu.VMEM(*n) for n in late_inputs + sizes]

time: 154 us -> 146 us (0.948)
  Pallas kernels: 152 us -> 144 us
    pallas_call x1, Pallas kernels: 152 us -> 144 us  [layer(): pl.pallas_call(layer_kernel, out_shape=jax.ShapeDtypeStruct((32, 4096), b...]
where the time goes in v1:
time: 146 us
  Pallas kernels  144 us (99%)
  local copies, waits for them, and re-layouts  1.67 us (1%)
    pallas_call x1, Pallas kernels, layer(): pl.pallas_call(layer_kernel, out_shape=jax.ShapeDtypeStruct((32, 4096), b...  144 us

profile of v1, /device:TPU:1, one launch (start us, length us, event | category | flops | bytes accessed | tf_op | source)
XLA Modules:
  0.0 145.9 jit_solution(17831388016090417546)
XLA Ops:
  0.0 144.2 %shard_map.127 = bf16[32,4096]{1,0:T(8,128)(2,1)} custom-call(bf16[128,512]{1,0:T(8,128)(2,1)} %q_hbm.1, bf16[128,128]{1,0:T(8,128)(2,1)} %k_hbm.1, bf16[128,128]{1,0:T(8,128)(2,1)} %v_hbm.1, f32[1,4]{1,0:T(1,128)} %bitcast.14, bf16[32,4096]{1,0:T(8,128)(2,1)} %res_hbm.1, bf16[512,4096]{1,0:T(8,128)(2,1)} %w_hbm.1, f32[1,4096]{1,0:T(1,128)} %bitcast.11, ...), custom_call_target="tpu_custom_call" | custom-call | tf_op jit(solution)/shard_map/pallas_call | solution.py:543
  144.2 1.7 %copy.15 = bf16[32,4096]{1,0:T(8,128)(2,1)} copy(bf16[32,4096]{1,0:T(8,128)(2,1)} %shard_map.127) | data formatting | bytes 524288

commit v2 on v1

--- a/solution.py
+++ b/solution.py
@@ -87,7 +87,7 @@
     return y, (y + 1) % 4, (y + 3) % 4, (y + 2) % 4
 
 
-OFFS = (0, -3, 3, 2, -2, 4, 1, -1)
+OFFS = (0, 3, -3, 2, -2, 4, 1, -1)
 
 
 def slot_columns(pick_ref, z):
@@ -96,15 +96,15 @@
     earlier = (lanes < rows) & ((lanes & 96) == (rows & 96))
     across = [jnp.broadcast_to(pick_ref[k : k + 1, :], (128, 128)) for k in range(2)]
     wide = [w.astype(jnp.float32).T.astype(jnp.int32) for w in across]
-    lane, late = [], []
+    place, chunks = [], []
     for w in wide:
         same = earlier & ((across[0] == w) | (across[1] == w))
         rank = jnp.sum(jnp.where(same, 1.0, 0.0), axis=1, keepdims=True).astype(jnp.int32)
         away = (z - (w >> 3)) & 7
         chunk = sum(jnp.where(away == (off & 7), o, 0) for o, off in enumerate(OFFS))
-        lane.append((w & 7) * 16 + (chunk & 3) * 2 + rank)
-        late.append(chunk >> 2)
-    return lane, late
+        place.append((w & 7) * 16 + rank)
+        chunks.append(chunk)
+    return place, chunks
 
 
 def layer_kernel(q_hbm, k_hbm, v_hbm, bias_hbm, res_hbm, w_hbm, gain_hbm, pick_hbm, logit_hbm, gate_hbm, up_hbm, down_ref, last_hbm,
@@ -322,12 +322,12 @@
     project(3)
     copies[1].start()
     copies[2].start()
-    lane, late = slot_columns(pick_ref, z)
+    spot, chunks = slot_columns(pick_ref, z)
     lanes = lax.broadcasted_iota(jnp.int32, (128, 128), 1)
-    for h in range(2):
-        for half in range(2):
-            hit = [(lane[k] + 8 * half == lanes) & (late[k] == h) for k in range(2)]
-            slots[h, half] = jnp.where(hit[0] | hit[1], 1.0, 0.0).astype(jnp.bfloat16)
+    for g in range(4):
+        for n in range(4):
+            hit = [(spot[k] + (chunks[k] & 1) * 2 + 4 * n == lanes) & ((chunks[k] >> 1) == g) for k in range(2)]
+            slots[g, n] = jnp.where(hit[0] | hit[1], 1.0, 0.0).astype(jnp.bfloat16)
     copies[0].wait_recv()
     summed[0] = (part[right, 0].astype(jnp.float32) + relay[0].astype(jnp.float32)).astype(jnp.bfloat16)
     copies[4].start()
@@ -365,32 +365,33 @@
 
     way_y = {"R": {"sp": sp, "tp": right}, "L": {"sp": sp, "tp": left}, "O": {"sp": sp, "tp": over}}
 
-    def pass_on_x(o, h):
+    def pass_on_x(o, g):
         zz, xx, cc = plane[o]
-        push(("x", o, h), disp_ref.at[h, xx * 2 + cc], recv_x.at[h, j], device(zz, xx, cc))
+        push(("x", o, g), disp_ref.at[g, xx * 2 + cc], recv_x.at[g, j], device(zz, xx, cc))
 
     own_rows = pl.ds(pl.multiple_of(y * 32, 32), 32)
-    f = [(stream_ref[:, n * 2048:(n + 1) * 2048].astype(jnp.float32) * scale * gain_ref[:, n * 2048:(n + 1) * 2048]).astype(jnp.bfloat16) for n in range(2)]
+    quarters = [slice(n * 1024, (n + 1) * 1024) for n in range(4)]
+    f = [(stream_ref[:, cols].astype(jnp.float32) * scale * gain_ref[:, cols]).astype(jnp.bfloat16) for cols in quarters]
     f = jnp.concatenate(f, axis=0)
-    for h in range(2):
-        mine = jnp.concatenate([slots[h, 0, own_rows, :], slots[h, 1, own_rows, :]], axis=0)
+    for g in range(4):
+        mine = jnp.concatenate([slots[g, n, own_rows, :] for n in range(4)], axis=0)
         d = lax.dot_general(mine, f, (((0,), (0,)), ((), ())), preferred_element_type=jnp.float32)
-        disp_ref[h] = d.astype(jnp.bfloat16).reshape(8, 16, 2048)
+        disp_ref[g] = d.astype(jnp.bfloat16).reshape(8, 16, 1024)
         for o in (4, 5, 2, 3, 6, 7, 1):
-            pass_on_x(o, h)
+            pass_on_x(o, g)
     loads["logit"].wait()
     logit = jnp.broadcast_to(logit_ref[...], (128, 128)).T
-    second = ((lax.broadcasted_iota(jnp.int32, (128, 128), 0) >> 5) & 1) * 8
+    block_of = ((lax.broadcasted_iota(jnp.int32, (128, 128), 0) >> 5) & 3) * 4
     chance = (jax.nn.sigmoid(logit), jax.nn.sigmoid(-logit))
-    for h in range(2):
-        w = sum(jnp.where((lane[k] + second == lanes) & (late[k] == h), chance[k], 0.0) for k in range(2))
+    for g in range(4):
+        w = sum(jnp.where((spot[k] + (chunks[k] & 1) * 2 + block_of == lanes) & ((chunks[k] >> 1) == g), chance[k], 0.0) for k in range(2))
         hi = w.astype(bf)
-        blend[:, h * 128:(h + 1) * 128] = hi
-        blend[:, 256 + h * 128:256 + (h + 1) * 128] = (w - hi.astype(f32)).astype(bf)
+        blend[:, g * 128:(g + 1) * 128] = hi
+        blend[:, 512 + g * 128:512 + (g + 1) * 128] = (w - hi.astype(f32)).astype(bf)
     a = lax.broadcasted_iota(jnp.int32, (128, 128), 0)
     b = lax.broadcasted_iota(jnp.int32, (128, 128), 1)
-    outward = [jnp.where(b == ((a >> 1) & 7) * 16 + half * 8 + ((a >> 4) & 3) * 2 + (a & 1), 1.0, 0.0).astype(bf)[0:64] for half in range(2)]
-    homeward = jnp.where(b == ((a >> 1) & 3) * 32 + ((a >> 3) & 1) * 16 + (a >> 4) * 2 + (a & 1), 1.0, 0.0).astype(bf)
+    outward = [jnp.where(b == ((a >> 1) & 7) * 16 + n * 4 + ((a >> 4) & 1) * 2 + (a & 1), 1.0, 0.0).astype(bf)[0:32] for n in range(4)]
+    homeward = jnp.where(b == ((a >> 1) & 1) * 64 + ((a >> 2) & 3) * 16 + (a >> 4) * 2 + (a & 1), 1.0, 0.0).astype(bf)
     halves = [slice(0, 2048), slice(2048, 4096)]
     plane_order = (1, 2, 3, 6, 7, 4, 5)
 
@@ -403,34 +404,39 @@
             for way in "RL":
                 push(("g", way, o, half), part, part, way_y[way])
 
-    def permute(h):
-        recv_x[h, j] = disp_ref[h, j]
+    def permute(g):
+        recv_x[g, j] = disp_ref[g, j]
         for o in plane_order:
-            arrive(("x", o, h), recv_x.at[h, place_of(o)])
-        v = recv_x[h].reshape(128, 2048)
-        for half in range(2):
-            p = jnp.dot(outward[half], v, preferred_element_type=f32).astype(bf).reshape(4, 16, 2048)
-            send_z[4 * h:4 * h + 4, :, halves[half]] = p
-            if h == 0:
-                got[0, y, :, halves[half]] = p[0]
-        for o in range(4 * h, 4 * h + 4):
+            arrive(("x", o, g), recv_x.at[g, place_of(o)])
+        v = recv_x[g].reshape(128, 1024)
+        for n in range(4):
+            p = jnp.dot(outward[n], v, preferred_element_type=f32).astype(bf).reshape(2, 16, 1024)
+            send_z[2 * g:2 * g + 2, :, quarters[n]] = p
+            if g == 0:
+                got[0, y, :, quarters[n]] = p[0]
+        for o in (2 * g, 2 * g + 1):
             if o:
                 push(("z", o), send_z.at[o], got.at[o, y], device((z - OFFS[o] + 8) % 8, x, c))
             else:
                 over_y(0)
 
+    def own(o):
+        arrive(("z", o), got.at[o, y])
+        over_y(o)
+
+    def on(o):
+        for h, way, t in ((0, "R", left), (1, "L", right)):
+            part = got.at[o, t, :, halves[h]]
+            arrive(("g", way, o, h), part)
+            push(("h", way, o), part, part, way_y[way])
+
     def gather_own(g):
-        for o in (2 * g, 2 * g + 1):
-            if o:
-                arrive(("z", o), got.at[o, y])
-                over_y(o)
+        own(2 * g)
+        own(2 * g + 1)
 
     def gather_on(g):
-        for o in (2 * g, 2 * g + 1):
-            for h, way, t in ((0, "R", left), (1, "L", right)):
-                part = got.at[o, t, :, halves[h]]
-                arrive(("g", way, o, h), part)
-                push(("h", way, o), part, part, way_y[way])
+        on(2 * g)
+        on(2 * g + 1)
 
     def hidden(g):
         for o in (2 * g, 2 * g + 1):
@@ -465,28 +471,31 @@
             else:
                 recv_r[0] = result[0]
 
-    def homeward_x(h):
-        for o in range(4 * h, 4 * h + 4):
+    def homeward_x(g):
+        for o in (2 * g, 2 * g + 1):
             if o:
                 arrive(("r", o), recv_r.at[o])
-        for t in range(2):
-            v = recv_r[4 * h:4 * h + 4, 2 * t:2 * t + 2].reshape(128, 1024)
-            p = jnp.dot(homeward, v, preferred_element_type=f32)
-            send_x[h, :, t] = p.astype(bf).reshape(8, 16, 1024)
+        v = recv_r[2 * g:2 * g + 2].reshape(128, 1024)
+        p = jnp.dot(homeward, v, preferred_element_type=f32)
+        send_x[g] = p.astype(bf).reshape(8, 16, 1024)
         for o in (4, 5, 2, 3, 6, 7, 1):
             zz, xx, cc = plane[o]
-            push(("b", o, h), send_x.at[h, xx * 2 + cc], recv_b.at[h, j], device(zz, xx, cc))
-        recv_b[h, j] = send_x[h, j]
+            push(("b", o, g), send_x.at[g, xx * 2 + cc], recv_b.at[g, j], device(zz, xx, cc))
+        recv_b[g, j] = send_x[g, j]
 
     permute(0)
     permute(1)
+    on(0)
+    permute(2)
+    own(1)
+    permute(3)
+    on(1)
     loads["gate"].wait()
     loads["up"].wait()
     loads["last"].wait()
-    gather_own(0)
     for p in range(4):
-        gather_on(p)
         if p > 0:
+            gather_on(p)
             hidden_on(p - 1)
         if p < 3:
             gather_own(p + 1)
@@ -497,20 +506,19 @@
     homeward_x(0)
     outputs(3)
     homeward_x(1)
-    for h in range(2):
+    homeward_x(2)
+    homeward_x(3)
+    for g in range(4):
         for o in plane_order:
-            arrive(("b", o, h), recv_b.at[h, place_of(o)])
-
-    def blended(t):
-        w = blend[pl.ds(pl.multiple_of(t * 32, 32), 32), :]
-        v = [recv_b[h, :, t // 2].reshape(128, 1024) for h in range(2)]
-        v = jnp.concatenate(v + v, axis=0)
-        return jnp.dot(w, v, preferred_element_type=f32).astype(bf)
-
+            arrive(("b", o, g), recv_b.at[g, place_of(o)])
+
+    v = recv_b[...].reshape(512, 1024)
+    blended = (jnp.dot(blend[:, 0:512], v, preferred_element_type=f32)
+               + jnp.dot(blend[:, 512:1024], v, preferred_element_type=f32))
+    send_f[...] = blended.astype(bf).reshape(4, 32, 1024)
     for way, t in (("O", over), ("R", right), ("L", left)):
-        send_f[t] = blended(t)
         push(("f", way), send_f.at[t], fin.at[y], way_y[way])
-    fin[y] = blended(y)
+    fin[y] = send_f[y]
     for way, t in (("R", left), ("L", right), ("O", over)):
         arrive(("f", way), fin.at[t])
     square = jnp.zeros((32, 1), f32)
@@ -533,17 +541,17 @@
     inputs = [((128, 512), bf), ((128, 128), bf), ((128, 128), bf)]
     late_inputs = [((32, 4096), bf), ((512, 4096), bf), ((1, 4096), f32), ((2, 128), jnp.int32), ((1, 128), f32),
                    ((4096, 256), bf), ((4096, 256), bf), ((1, 4096), f32)]
-    sizes = [((32, 4096), bf), ((2, 8, 16, 2048), bf), ((4, 256, 1024), bf),
+    sizes = [((32, 4096), bf), ((4, 8, 16, 1024), bf), ((4, 256, 1024), bf),
              ((2, 32, 128, 128), bf), ((2, 32, 128, 128), bf), ((512, 128), bf), ((KB, KB), bf), ((512, 128), f32),
              ((512, 128), f32), ((128, 512), bf), ((2, 128, 1024), bf), ((4, 2, 32, 2048), bf),
-             ((2, 32, 2048), bf), ((2, 32, 2048), bf), ((2, 32, 2048), bf), ((2, 32, 2048), bf), ((2, 2, 128, 128), bf),
-             ((2, 8, 16, 2048), bf), ((8, 16, 4096), bf), ((8, 4, 16, 4096), bf), ((4, 4, 128, 256), bf), ((8, 4, 16, 1024), bf),
-             ((8, 4, 16, 1024), bf), ((2, 8, 2, 16, 1024), bf), ((2, 8, 2, 16, 1024), bf), ((128, 512), bf), ((4, 32, 1024), bf),
+             ((2, 32, 2048), bf), ((2, 32, 2048), bf), ((2, 32, 2048), bf), ((2, 32, 2048), bf), ((4, 4, 128, 128), bf),
+             ((4, 8, 16, 1024), bf), ((8, 16, 4096), bf), ((8, 4, 16, 4096), bf), ((4, 4, 128, 256), bf), ((8, 4, 16, 1024), bf),
+             ((8, 4, 16, 1024), bf), ((4, 8, 16, 1024), bf), ((4, 8, 16, 1024), bf), ((128, 1024), bf), ((4, 32, 1024), bf),
              ((4, 32, 1024), bf), ((512, 128), f32)]
     return pl.pallas_call(
         layer_kernel, out_shape=jax.ShapeDtypeStruct((32, 4096), bf), in_specs=[hbm] * 13, out_specs=vm,
         scratch_shapes=[pltpu.VMEM(*n) for n in inputs] + [pltpu.SMEM((1, 4), f32)] + [pltpu.VMEM(*n) for n in late_inputs + sizes]
-        + [dma((126,)), dma((126,)), dma((6,)), dma((6,)), dma((6,)), dma((6,)), dma((112,)), dma((112,)), dma((13,))],
+        + [dma((126,)), dma((126,)), dma((6,)), dma((6,)), dma((6,)), dma((6,)), dma((144,)), dma((144,)), dma((13,))],
         compiler_params=pltpu.CompilerParams(collective_id=0, has_side_effects=True, vmem_limit_bytes=60 * 1024 * 1024),
     )(*args)
 

time: 146 us -> 142 us (0.973)
  Pallas kernels: 144 us -> 140 us
    pallas_call x1, Pallas kernels: 144 us -> 140 us  [layer(): pl.pallas_call(layer_kernel, out_shape=jax.ShapeDtypeStruct((32, 4096), b...]
where the time goes in v2:
time: 142 us
  Pallas kernels  140 us (99%)
  local copies, waits for them, and re-layouts  1.67 us (1%)
    pallas_call x1, Pallas kernels, layer(): pl.pallas_call(layer_kernel, out_shape=jax.ShapeDtypeStruct((32, 4096), b...  140 us

profile of v2, /device:TPU:1, one launch (start us, length us, event | category | flops | bytes accessed | tf_op | source)
XLA Modules:
  0.0 141.6 jit_solution(14978763159810466507)
XLA Ops:
  0.0 139.9 %shard_map.127 = bf16[32,4096]{1,0:T(8,128)(2,1)} custom-call(bf16[128,512]{1,0:T(8,128)(2,1)} %q_hbm.1, bf16[128,128]{1,0:T(8,128)(2,1)} %k_hbm.1, bf16[128,128]{1,0:T(8,128)(2,1)} %v_hbm.1, f32[1,4]{1,0:T(1,128)} %bitcast.14, bf16[32,4096]{1,0:T(8,128)(2,1)} %res_hbm.1, bf16[512,4096]{1,0:T(8,128)(2,1)} %w_hbm.1, f32[1,4096]{1,0:T(1,128)} %bitcast.11, ...), custom_call_target="tpu_custom_call" | custom-call | tf_op jit(solution)/shard_map/pallas_call | solution.py:551
  139.9 1.7 %copy.15 = bf16[32,4096]{1,0:T(8,128)(2,1)} copy(bf16[32,4096]{1,0:T(8,128)(2,1)} %shard_map.127) | data formatting | bytes 524288
